TPU v7x, 32 devices: a whole 2x2x4 slice. The times are simulated.
32 devices in a mesh: sp: 8 (over z, x), tp: 4 (over y, core).
Axes of the slice: x: 2, y: 2, z: 4, core: 2. Of those that a mesh axis runs over, the one named last changes fastest.
Arguments:
- residual_signal: bfloat16 [1024, 2048], P('sp', 'tp'), may hold values from -90 to 90
- lifted_signal: bfloat16 [1024, 1024], P('sp', 'tp'), may hold values from -6 to 6
- discrete_timestep: float32 [64, 1024], P('tp', 'sp'), may hold values from 0.17 to 4.2
- additional_log_fading: float32 [64, 1024], P('tp', 'sp'), may hold values from -2.1 to 0
- paired_fading: float32 [2, 32, 64], replicated, may hold values from 1.953125e-05 to 0.0625
- unpaired_fading: float32 [2, 32, 32], replicated, may hold values from 1.953125e-05 to 0.0625
- paired_twist: float32 [2, 32, 64], replicated, may hold values from -3.140625 to 3.140625
- unpaired_twist: float32 [2, 32, 32], replicated, may hold values from -3.140625 to 3.140625
- paired_latent_linears: float32 [2, 2, 2, 32, 64, 16], replicated, may hold values from -1 to 1
- unpaired_latent_linears: float32 [2, 2, 2, 32, 32, 16], replicated, may hold values from -1 to 1
- skip_coefficient: float32 [1024], replicated, may hold values from -4 to 4
- closing_norm_multiplier: float32 [1024], replicated, may hold values from 0.1 to 1.9
- emitted_linear: bfloat16 [1024, 2048], replicated, may hold values from -0.1875 to 0.1875
- leading_norm_multiplier: float32 [2048], replicated, may hold values from 0.1 to 1.9
- raising_linear: bfloat16 [2048, 8192], P('sp', 'tp'), may hold values from -0.125 to 0.125
- lowering_linear: bfloat16 [8192, 2048], P('tp', 'sp'), may hold values from -0.0625 to 0.0625
Outputs:
- layer_out: bfloat16 [1024, 2048], P('sp', 'tp')
All inputs are finite; a program needn't handle non-finite values.
Results may differ from a plain program's by a relative error of at most 0.008.
Values may be sent and summed in bfloat16 or wider, within the bound.
No kernel may reach another device: no remote copies, remote signals or barrier semaphores. Data moves between devices by JAX's collectives and lax.ppermute only.
A program may use at most 128 MiB of HBM per device.

v0:
```python
import jax
import jax.numpy as jnp
from jax import lax
from jax.experimental import pallas as pl
from jax.experimental.pallas import tpu as pltpu
from jax.sharding import Mesh
from jax.sharding import PartitionSpec as P

CHAN = 16
NORM_W = 128
CHUNKS = 8
LANES = 128
EPSILON = 1e-06
HALVES = 2
SIN = (3.1415926532428884, -5.167712741152494, 2.5501627931734125, -0.5992473907509345, 0.08203117351788075, -0.00700041798679132)
COS = (0.9999999997799042, -4.934802137078826, 4.058709159556303, -1.33521200305024, 0.23493731381503577, -0.02439632434807213)
FADE = (1.0, -1.0 / 2, 1.0 / 6, -1.0 / 24, 1.0 / 120, -1.0 / 720, 1.0 / 5040, -1.0 / 40320)
F32 = jnp.float32
BF16 = jnp.bfloat16


def horner(coefficients, x):
    total = jnp.full_like(x, coefficients[-1])
    for c in coefficients[-2::-1]:
        total = total * x + c
    return total


def sin_cos(angle):
    halves = angle * 0.3183098861837907
    whole = jnp.round(halves)
    r = halves - whole
    z = r * r
    odd = whole * 0.5
    odd = odd - jnp.floor(odd)
    sign = 1.0 - 4.0 * odd
    return sign * r * horner(SIN, z), sign * horner(COS, z)


def one_minus_exp(z):
    return jnp.where(z < 0.5, z * horner(FADE, z), 1.0 - jnp.exp(-z))


def iota(shape, axis):
    return lax.broadcasted_iota(jnp.int32, shape, axis)


def time_of_row(row, tokens, backward):
    steps = tokens // CHUNKS
    t = (row % CHUNKS) * steps + row // CHUNKS
    return tokens - 1 - t if backward else t


def group_of_lane(lane, pairs, long_states, short_states):
    border = pairs * long_states
    return jnp.where(
        lane < border,
        2 * (lane // long_states),
        2 * ((lane - border) // short_states) + 1,
    )


def tiled(part, copies):
    return jnp.concatenate([part] * copies, axis=-1) if copies > 1 else part


def spread(long_part, short_part):
    pairs, chan, long_states = long_part.shape
    short_states = short_part.shape[2]
    rows = pairs * 2 * chan
    long_rows = jnp.concatenate([long_part, jnp.zeros_like(long_part)], axis=1)
    short_rows = jnp.concatenate([jnp.zeros_like(short_part), short_part], axis=1)
    halves = []
    for part, states in ((long_rows, long_states), (short_rows, short_states)):
        part = part.reshape(rows, states)
        part = tiled(part, LANES // states)
        part = tiled(part, pairs * states // LANES)
        keep = iota(part.shape, 1) // states == iota(part.shape, 0) // (2 * chan)
        halves.append(jnp.where(keep, part, 0.0))
    return jnp.concatenate(halves, axis=1).astype(BF16)


def flat_row(long_part, short_part):
    halves = []
    for part in (long_part, short_part):
        pairs, states = part.shape
        wide = tiled(tiled(part, LANES // states), pairs * states // LANES)
        keep = iota(wide.shape, 1) // states == iota(wide.shape, 0)
        halves.append(jnp.sum(jnp.where(keep, wide, 0.0), axis=0, keepdims=True))
    return jnp.concatenate(halves, axis=1)


def three_parts(x):
    high = x.astype(BF16).astype(F32)
    rest = x - high
    middle = rest.astype(BF16).astype(F32)
    return [high, middle, rest - middle]


def scan_kernel(
    rank_ref, input_ref, pace_ref, surge_ref, long_rate_ref, short_rate_ref, long_turn_ref, short_turn_ref,
    long_maps_ref, short_maps_ref, maps_ref, ends_ref, tail_ref,
):
    tokens, width = input_ref.shape
    groups = pace_ref.shape[0]
    _, pairs, long_states = long_rate_ref.shape
    short_states = short_rate_ref.shape[2]
    lanes = pairs * (long_states + short_states)
    steps = tokens // CHUNKS
    pieces = three_parts(pace_ref[...]) + three_parts(surge_ref[...])
    six = jnp.concatenate(pieces, axis=0).astype(BF16)
    inputs = input_ref[...]
    row = iota((6 * groups, lanes), 0)
    owner = group_of_lane(iota((6 * groups, lanes), 1), pairs, long_states, short_states)
    match = row % groups == owner
    pace_map = jnp.where(match & (row < 3 * groups), 1.0, 0.0).astype(BF16)
    surge_map = jnp.where(match & (row >= 3 * groups), 1.0, 0.0).astype(BF16)
    for d in range(2):
        place = time_of_row(iota((tokens, tokens), 0), tokens, d == 1) == iota((tokens, tokens), 1)
        place = jnp.where(place, 1.0, 0.0).astype(BF16)
        ordered = jnp.dot(place, inputs, preferred_element_type=F32).astype(BF16)
        six_rows = lax.dot_general(
            place, six, (((1,), (1,)), ((), ())), preferred_element_type=F32
        ).astype(BF16)
        rate = flat_row(long_rate_ref[d], short_rate_ref[d])
        turn = flat_row(long_turn_ref[d], short_turn_ref[d])
        in_re = spread(long_maps_ref[d, 0, 0], short_maps_ref[d, 0, 0])
        in_im = spread(long_maps_ref[d, 0, 1], short_maps_ref[d, 0, 1])
        for at in range(0, lanes, LANES):
            block = slice(at, at + LANES)
            pace = jnp.dot(six_rows, pace_map[:, block], preferred_element_type=F32)
            surge = jnp.dot(six_rows, surge_map[:, block], preferred_element_type=F32)
            fall = rate[:, block] * pace
            size = jnp.exp(surge - fall)
            sin, cos = sin_cos(turn[:, block] * pace)
            by_re, by_im = size * cos, size * sin
            weight = jnp.sqrt(one_minus_exp(2.0 * fall))
            add_re = jnp.dot(ordered, in_re[:, block], preferred_element_type=F32) * weight
            add_im = jnp.dot(ordered, in_im[:, block], preferred_element_type=F32) * weight
            for k in range(steps):
                rows = slice(CHUNKS * k, CHUNKS * (k + 1))
                b_re, b_im, a_re, a_im = by_re[rows], by_im[rows], add_re[rows], add_im[rows]
                if k == 0:
                    p_re, p_im, s_re, s_im = b_re, b_im, a_re, a_im
                else:
                    p_re, p_im = b_re * p_re - b_im * p_im, b_re * p_im + b_im * p_re
                    s_re, s_im = b_re * s_re - b_im * s_im + a_re, b_re * s_im + b_im * s_re + a_im
                maps_ref[d, 0, rows, block] = p_re
                maps_ref[d, 1, rows, block] = p_im
                maps_ref[d, 2, rows, block] = s_re
                maps_ref[d, 3, rows, block] = s_im
            for i, part in enumerate((p_re, p_im, s_re, s_im)):
                tail_ref[i, :, block] = part
        total = [tail_ref[i, 0:1, :] for i in range(4)]
        for c in range(1, CHUNKS):
            p_re, p_im, s_re, s_im = (tail_ref[i, c : c + 1, :] for i in range(4))
            t_re, t_im, e_re, e_im = total
            total = [
                p_re * t_re - p_im * t_im,
                p_re * t_im + p_im * t_re,
                p_re * e_re - p_im * e_im + s_re,
                p_re * e_im + p_im * e_re + s_im,
            ]
        for i in range(4):
            ends_ref[4 * d + i : 4 * d + i + 1, :] = total[i]


def settle_kernel(
    place_ref, maps_ref, ends_ref, input_ref, skip_ref, gain_ref, long_maps_ref, short_maps_ref, merged_ref, carry_ref
):
    tokens, width = input_ref.shape
    lanes = maps_ref.shape[3]
    steps = tokens // CHUNKS
    members = ends_ref.shape[0]
    me = place_ref[1]
    total = jnp.zeros((tokens, width), F32)
    for d in range(2):
        c_re = jnp.zeros((1, lanes), F32)
        c_im = jnp.zeros((1, lanes), F32)
        order = range(members - 1, -1, -1) if d else range(members)
        for s in order:
            p_re, p_im, s_re, s_im = (ends_ref[s, 4 * d + i : 4 * d + i + 1, :] for i in range(4))
            reached = (s > me) if d else (s < me)
            n_re = p_re * c_re - p_im * c_im + s_re
            n_im = p_re * c_im + p_im * c_re + s_im
            c_re = jnp.where(reached, n_re, c_re)
            c_im = jnp.where(reached, n_im, c_im)
        last = CHUNKS * (steps - 1)
        for c in range(CHUNKS):
            carry_ref[0, c : c + 1, :] = c_re
            carry_ref[1, c : c + 1, :] = c_im
            p_re, p_im, s_re, s_im = (maps_ref[d, i, last + c : last + c + 1, :] for i in range(4))
            c_re, c_im = p_re * c_re - p_im * c_im + s_re, p_re * c_im + p_im * c_re + s_im
        out_re = spread(long_maps_ref[d, 1, 0], short_maps_ref[d, 1, 0])
        out_im = spread(long_maps_ref[d, 1, 1], short_maps_ref[d, 1, 1])
        read = jnp.zeros((tokens, width), F32)
        for at in range(0, lanes, LANES):
            block = slice(at, at + LANES)
            e_re = jnp.concatenate([carry_ref[0, :, block]] * steps, axis=0)
            e_im = jnp.concatenate([carry_ref[1, :, block]] * steps, axis=0)
            p_re, p_im = maps_ref[d, 0, :, block], maps_ref[d, 1, :, block]
            state_re = maps_ref[d, 2, :, block] + p_re * e_re - p_im * e_im
            state_im = maps_ref[d, 3, :, block] + p_re * e_im + p_im * e_re
            contract = (((1,), (1,)), ((), ()))
            read += lax.dot_general(
                state_re.astype(BF16), out_re[:, block], contract, preferred_element_type=F32
            )
            read -= lax.dot_general(
                state_im.astype(BF16), out_im[:, block], contract, preferred_element_type=F32
            )
        place = time_of_row(iota((tokens, tokens), 1), tokens, d == 1) == iota((tokens, tokens), 0)
        place = jnp.where(place, 1.0, 0.0).astype(BF16)
        high = read.astype(BF16)
        low = (read - high.astype(F32)).astype(BF16)
        total += jnp.dot(place, high, preferred_element_type=F32)
        total += jnp.dot(place, low, preferred_element_type=F32)
    active = jax.nn.gelu(total + skip_ref[...] * input_ref[...].astype(F32))
    for at in range(0, width, NORM_W):
        block = slice(at, at + NORM_W)
        part = active[:, block]
        part = part * lax.rsqrt(jnp.mean(part * part, axis=1, keepdims=True) + EPSILON)
        merged_ref[:, block] = (part * gain_ref[:, block]).astype(BF16)


def project_kernel(place_ref, merged_ref, residual_ref, emit_ref, gain_ref, normed_ref, own_ref):
    _, members, tokens, width = merged_ref.shape
    features = residual_ref.shape[3]
    depth = members * features
    projected = jnp.zeros((tokens, depth), F32)
    for t in range(members):
        projected += jnp.dot(
            merged_ref[0, t], emit_ref[t * width : (t + 1) * width, :], preferred_element_type=F32
        )
    middle = projected + jnp.concatenate(
        [residual_ref[0, t].astype(F32) for t in range(members)], axis=1
    )
    scale = lax.rsqrt(jnp.mean(middle * middle, axis=1, keepdims=True) + EPSILON)
    normed_ref[...] = (middle * scale * gain_ref[...]).astype(BF16)
    for t in range(members):

        @pl.when((place_ref[0] == t) & (place_ref[2] == pl.program_id(0)))
        def _(t=t):
            own_ref[...] = middle[:, t * features : (t + 1) * features]


def feed_kernel(normed_ref, raise_ref, lower_ref, out_ref):
    members, features = out_ref.shape[1], out_ref.shape[3]
    upward = jnp.dot(normed_ref[...], raise_ref[...], preferred_element_type=F32)
    hidden = jnp.square(jnp.maximum(upward, 0.0)).astype(BF16)
    parts = [
        jnp.dot(hidden, lower_ref[s], preferred_element_type=F32).astype(BF16)
        for s in range(lower_ref.shape[0])
    ]
    whole = jnp.concatenate(parts, axis=1) if len(parts) > 1 else parts[0]
    for t in range(members):
        out_ref[0, t] = whole[:, t * features : (t + 1) * features]


def exchange(x, axes):
    return lax.all_to_all(x, axes, split_axis=0, concat_axis=0, tiled=True)


def everywhere(x, axes, members):
    return exchange(jnp.broadcast_to(x[None], (members,) + x.shape), axes)


def params(**more):
    return pltpu.CompilerParams(vmem_limit_bytes=56 * 1024 * 1024, **more)


def on_device(
    residual_signal, lifted_signal, discrete_timestep, additional_log_fading, paired_fading, unpaired_fading,
    paired_twist, unpaired_twist, paired_latent_linears, unpaired_latent_linears, skip_coefficient,
    closing_norm_multiplier, emitted_linear, leading_norm_multiplier, raising_linear, lowering_linear,
):
    members = lax.axis_size("tp")
    inner = lax.axis_size("q")
    line = HALVES * inner
    rank = lax.axis_index("tp")
    my_q = lax.axis_index("q")
    me = lax.axis_index("zh") * inner + my_q
    place = jnp.stack([rank, me, my_q]).astype(jnp.int32)
    tokens, width = lifted_signal.shape
    groups = discrete_timestep.shape[0]
    pairs = groups // 2
    long_states, short_states = paired_fading.shape[2], unpaired_fading.shape[2]
    lanes = pairs * (long_states + short_states)
    depth_rows, hidden_columns = raising_linear.shape
    depth = depth_rows * line
    features = residual_signal.shape[1]
    share = hidden_columns // inner

    raise_parts = raising_linear.reshape(depth_rows, inner, share).transpose(1, 0, 2)
    raise_parts = jnp.concatenate([raise_parts] * HALVES, axis=0)
    lower_parts = lowering_linear.reshape(inner, share, depth_rows)
    lower_parts = jnp.concatenate([lower_parts] * HALVES, axis=0)
    raised = exchange(raise_parts, ("zh", "q")).reshape(depth, share)
    lowered = exchange(lower_parts, ("zh", "q"))
    if depth_rows % LANES:
        lowered = lowered.transpose(1, 0, 2).reshape(1, share, depth)
    residual_all = everywhere(residual_signal, ("q", "tp"), inner * members).reshape(
        inner, members, tokens, features
    )

    long_maps = jnp.swapaxes(paired_latent_linears, 4, 5)
    short_maps = jnp.swapaxes(unpaired_latent_linears, 4, 5)

    def owned(*shape, at):
        return pl.BlockSpec(shape, lambda i, place_ref: tuple(place_ref[0] if k == at else 0 for k in range(len(shape))))

    def rates(states):
        return pl.BlockSpec((2, None, pairs, states), lambda i, place_ref: (0, place_ref[0], 0, 0))

    def by_rank(array):
        return array.reshape(2, members, pairs, array.shape[2])

    def full(*shape):
        return pl.BlockSpec(shape, lambda i, place_ref: (0,) * len(shape))

    long_spec = owned(2, 2, 2, pairs, CHAN, long_states, at=3)
    short_spec = owned(2, 2, 2, pairs, CHAN, short_states, at=3)
    maps, ends = pl.pallas_call(
        scan_kernel,
        grid_spec=pltpu.PrefetchScalarGridSpec(
            num_scalar_prefetch=1,
            grid=(1,),
            in_specs=[
                full(tokens, width),
                full(groups, tokens),
                full(groups, tokens),
                rates(long_states),
                rates(short_states),
                rates(long_states),
                rates(short_states),
                long_spec,
                short_spec,
            ],
            out_specs=[full(2, 4, tokens, lanes), full(8, lanes)],
            scratch_shapes=[pltpu.VMEM((4, CHUNKS, lanes), F32)],
        ),
        out_shape=[
            jax.ShapeDtypeStruct((2, 4, tokens, lanes), F32),
            jax.ShapeDtypeStruct((8, lanes), F32),
        ],
        compiler_params=params(),
        name="scan",
    )(
        place, lifted_signal, discrete_timestep, additional_log_fading, by_rank(paired_fading),
        by_rank(unpaired_fading), by_rank(paired_twist), by_rank(unpaired_twist), long_maps, short_maps,
    )
    all_ends = everywhere(ends, ("zh", "q"), line)
    merged = pl.pallas_call(
        settle_kernel,
        grid_spec=pltpu.PrefetchScalarGridSpec(
            num_scalar_prefetch=1,
            grid=(1,),
            in_specs=[
                full(2, 4, tokens, lanes),
                full(line, 8, lanes),
                full(tokens, width),
                owned(1, width, at=1),
                owned(1, width, at=1),
                long_spec,
                short_spec,
            ],
            out_specs=full(tokens, width),
            scratch_shapes=[pltpu.VMEM((2, CHUNKS, lanes), F32)],
        ),
        out_shape=jax.ShapeDtypeStruct((tokens, width), BF16),
        compiler_params=params(),
        name="settle",
    )(
        place, maps, all_ends, lifted_signal, skip_coefficient[None], closing_norm_multiplier[None],
        long_maps, short_maps,
    )
    merged_all = everywhere(merged, ("q", "tp"), inner * members).reshape(inner, members, tokens, width)

    normed, own = pl.pallas_call(
        project_kernel,
        grid_spec=pltpu.PrefetchScalarGridSpec(
            num_scalar_prefetch=1,
            grid=(inner,),
            in_specs=[
                pl.BlockSpec((1, members, tokens, width), lambda i, place_ref: (i, 0, 0, 0)),
                pl.BlockSpec((1, members, tokens, features), lambda i, place_ref: (i, 0, 0, 0)),
                full(members * width, depth),
                full(1, depth),
            ],
            out_specs=[
                pl.BlockSpec((tokens, depth), lambda i, place_ref: (i, 0)),
                full(tokens, features),
            ],
        ),
        out_shape=[
            jax.ShapeDtypeStruct((inner * tokens, depth), BF16),
            jax.ShapeDtypeStruct((tokens, features), F32),
        ],
        compiler_params=params(),
        name="project",
    )(place, merged_all, residual_all, emitted_linear, leading_norm_multiplier[None])

    partial = pl.pallas_call(
        feed_kernel,
        grid=(inner,),
        in_specs=[
            pl.BlockSpec((tokens, depth), lambda i: (i, 0)),
            pl.BlockSpec((depth, share), lambda i: (0, 0)),
            pl.BlockSpec(lowered.shape, lambda i: (0, 0, 0)),
        ],
        out_specs=pl.BlockSpec((1, members, tokens, features), lambda i: (i, 0, 0, 0)),
        out_shape=jax.ShapeDtypeStruct((inner, members, tokens, features), BF16),
        compiler_params=params(),
        name="feed",
    )(normed, raised, lowered)
    shares = exchange(partial.reshape(inner * members, tokens, features), ("q", "tp"))
    return (own + jnp.sum(shares.astype(F32), axis=0)).astype(BF16)


def solution(mesh):
    sp, tp = mesh.axis_names
    line, members = mesh.shape[sp], mesh.shape[tp]
    split = Mesh(mesh.devices.reshape(HALVES, line // HALVES, members), ("zh", "q", "tp"))
    s, t = ("zh", "q"), "tp"
    in_specs = (P(s, t), P(s, t), P(t, s), P(t, s)) + (P(),) * 10 + (P(s, t), P(t, s))
    return jax.shard_map(
        on_device, mesh=split, in_specs=in_specs, out_specs=P(s, t), check_vma=False
    )
```

profile of v0, /device:TPU:0, one launch (start us, length us, event | category | flops | bytes accessed | tf_op | source)
XLA Modules:
  0.0 230.0 jit_solution(2947852695684202258)
XLA Ops:
  0.0 0.6 pad_add_fusion.rank_ref.place_ref
  0.6 6.7 %scan.1 = (f32[2,4,128,768]{3,2,1,0:T(8,128)}, f32[8,768]{1,0:T(8,128)}) custom-call(s32[3]{0:T(128)} %pad_add_fusion.rank_ref.place_ref, bf16[128,256]{1,0:T(8,128)(2,1)} %input_ref.3, f32[16,128]{1,0:T(8,128)} %pace_ref.1, f32[16,128]{1,0:T(8,128)} %surge_ref.1, f32[2,4,8,64]{3,2,1,0:T(8,128)} %bitcast.35, f32[2,4,8,32]{3,2,1,0:T(8,128)} %bitcast.36, ...), custom_call_target="tpu_custom_call" | custom-call | tf_op jit(solution)/shard_map/scan/pallas_call | solution.py:322
  7.3 0.8 broadcast_in_dim.12
  8.0 15.1 %all_to_all.30.ends_ref = f32[8,8,768]{2,1,0:T(8,128)} all-to-all(f32[8,8,768]{2,1,0:T(8,128)S(1)} %broadcast_in_dim.12), channel_id=1, replica_groups=mesh['zh'=2,'q'=4,'tp'=4] {'zh','q'}, dimensions={0} | all-to-all | bytes 393216 | tf_op jit(solution)/shard_map/all_to_all | solution.py:260
  23.2 4.9 %settle.1 = bf16[128,256]{1,0:T(8,128)(2,1)} custom-call(s32[3]{0:T(128)} %pad_add_fusion.rank_ref.place_ref, f32[2,4,128,768]{3,2,1,0:T(8,128)} %get-tuple-element.9.maps_ref, f32[8,8,768]{2,1,0:T(8,128)} %all_to_all.30.ends_ref, bf16[128,256]{1,0:T(8,128)(2,1)} %input_ref.3, f32[1,1024]{1,0:T(1,128)} %bitcast.40, f32[1,1024]{1,0:T(1,128)} %bitcast.41, ...), custom_call_target="tpu_custom_call" | custom-call | tf_op jit(solution)/shard_map/settle/pallas_call | solution.py:352
  28.1 0.0 copy-start.3
  28.1 2.0 broadcast_in_dim.30
  30.1 3.7 %all-to-all-start.1 = ((bf16[16,128,256]{2,1,0:T(8,128)(2,1)}), bf16[16,128,256]{2,1,0:T(8,128)(2,1)S(1)}, u32[]{:S(2)}, u32[]{:S(2)}) async-start(bf16[16,128,256]{2,1,0:T(8,128)(2,1)} %broadcast_in_dim.30), calls=%async_computation.1 | async-start | bytes 2097152 | tf_op jit(solution)/shard_map/all_to_all | solution.py:260
  33.7 0.0 copy-done.3
  33.7 0.1 copy.20
  33.8 0.2 pad_maximum_fusion
  34.0 0.0 copy-start.5
  34.0 15.8 %all-to-all-done.1 = bf16[16,128,256]{2,1,0:T(8,128)(2,1)S(1)} async-done(((bf16[16,128,256]{2,1,0:T(8,128)(2,1)}), bf16[16,128,256]{2,1,0:T(8,128)(2,1)S(1)}, u32[]{:S(2)}, u32[]{:S(2)}) %all-to-all-start.1) | async-done | bytes 1048608 | tf_op jit(solution)/shard_map/all_to_all | solution.py:260
  49.9 0.0 copy-start.1
  49.9 51.4 %all_to_all.31 = bf16[8,256,512]{2,1,0:T(8,128)(2,1)} all-to-all(bf16[8,256,512]{2,1,0:T(8,128)(2,1)S(1)} %pad_maximum_fusion), channel_id=1, replica_groups=mesh['zh'=2,'q'=4,'tp'=4] {'zh','q'}, dimensions={0} | all-to-all | bytes 4194304 | tf_op jit(solution)/shard_map/all_to_all | solution.py:260
  101.2 0.0 copy-done.5
  101.2 1.5 broadcast_in_dim.31
  102.8 0.0 copy-done.1
  102.8 0.0 copy-start.2
  102.8 3.8 %all-to-all-start.2 = ((bf16[16,128,512]{2,1,0:T(8,128)(2,1)}), bf16[16,128,512]{2,1,0:T(8,128)(2,1)S(1)}, u32[]{:S(2)}, u32[]{:S(2)}) async-start(bf16[16,128,512]{2,1,0:T(8,128)(2,1)} %broadcast_in_dim.31), calls=%async_computation.2 | async-start | bytes 4194304 | tf_op jit(solution)/shard_map/all_to_all | solution.py:260
  106.6 0.0 copy-done.2
  106.6 1.5 pad_maximum_fusion.1
  108.2 28.1 %all-to-all-done.2 = bf16[16,128,512]{2,1,0:T(8,128)(2,1)S(1)} async-done(((bf16[16,128,512]{2,1,0:T(8,128)(2,1)}), bf16[16,128,512]{2,1,0:T(8,128)(2,1)S(1)}, u32[]{:S(2)}, u32[]{:S(2)}) %all-to-all-start.2) | async-done | bytes 2097184 | tf_op jit(solution)/shard_map/all_to_all | solution.py:260
  136.3 0.0 copy-start
  136.3 1.4 copy-done
  137.6 4.3 %all-to-all-start.4 = ((bf16[8,512,256]{2,1,0:T(8,128)(2,1)}), bf16[8,512,256]{2,1,0:T(8,128)(2,1)}, u32[]{:S(2)}, u32[]{:S(2)}) async-start(bf16[8,512,256]{2,1,0:T(8,128)(2,1)} %pad_maximum_fusion.1), calls=%async_computation.4 | async-start | bytes 4194304 | tf_op jit(solution)/shard_map/all_to_all | solution.py:260
  142.0 8.2 %project.1 = (bf16[512,2048]{1,0:T(8,128)(2,1)}, f32[128,512]{1,0:T(8,128)}) custom-call(s32[3]{0:T(128)} %pad_add_fusion.rank_ref.place_ref, bf16[4,4,128,256]{3,2,1,0:T(8,128)(2,1)} %bitcast.32, bf16[4,4,128,512]{3,2,1,0:T(8,128)(2,1)} %bitcast.28, bf16[1024,2048]{1,0:T(8,128)(2,1)} %emit_ref.1, f32[1,2048]{1,0:T(1,128)} %bitcast.39), custom_call_target="tpu_custom_call" | custom-call | tf_op jit(solution)/shard_map/project/pallas_call | solution.py:378
  150.2 40.0 %all-to-all-done.4.lower_ref = bf16[8,512,256]{2,1,0:T(8,128)(2,1)} async-done(((bf16[8,512,256]{2,1,0:T(8,128)(2,1)}), bf16[8,512,256]{2,1,0:T(8,128)(2,1)}, u32[]{:S(2)}, u32[]{:S(2)}) %all-to-all-start.4) | async-done | bytes 2097184 | tf_op jit(solution)/shard_map/all_to_all | solution.py:260
  190.2 7.1 %feed.1 = bf16[4,4,128,512]{3,2,1,0:T(8,128)(2,1)} custom-call(bf16[512,2048]{1,0:T(8,128)(2,1)} %get-tuple-element.12.normed_ref, bf16[2048,512]{1,0:T(8,128)(2,1)} %bitcast.29, bf16[8,512,256]{2,1,0:T(8,128)(2,1)} %all-to-all-done.4.lower_ref), custom_call_target="tpu_custom_call" | custom-call | tf_op jit(solution)/shard_map/feed/pallas_call | solution.py:402
  197.3 31.0 %all_to_all.32 = bf16[16,128,512]{2,1,0:T(8,128)(2,1)S(1)} all-to-all(bf16[16,128,512]{2,1,0:T(8,128)(2,1)} %bitcast.30), channel_id=1, replica_groups=mesh['zh'=2,'q'=4,'tp'=4] {'q','tp'}, dimensions={0} | all-to-all | bytes 4194304 | tf_op jit(solution)/shard_map/all_to_all | solution.py:260
  228.3 0.0 copy-start.4
  228.3 0.3 convert_reduce_fusion
  228.6 0.7 copy-done.4
  229.3 0.7 add_convert_fusion
Async XLA Ops:
  28.1 5.7 %copy-start.3 = (bf16[256,2048]{1,0:T(8,128)(2,1)S(1)}, bf16[256,2048]{1,0:T(8,128)(2,1)}, u32[]{:S(2)}) copy-start(bf16[256,2048]{1,0:T(8,128)(2,1)} %param.30) | copy-start | bytes 3145732
  30.1 19.8 %all-to-all-start.1 = ((bf16[16,128,256]{2,1,0:T(8,128)(2,1)}), bf16[16,128,256]{2,1,0:T(8,128)(2,1)S(1)}, u32[]{:S(2)}, u32[]{:S(2)}) async-start(bf16[16,128,256]{2,1,0:T(8,128)(2,1)} %broadcast_in_dim.30), calls=%async_computation.1 | async-start | bytes 2097152 | tf_op jit(solution)/shard_map/all_to_all | solution.py:260
  34.0 67.2 %copy-start.5 = (bf16[128,512]{1,0:T(8,128)(2,1)S(1)}, bf16[128,512]{1,0:T(8,128)(2,1)}, u32[]{:S(2)}) copy-start(bf16[128,512]{1,0:T(8,128)(2,1)} %param.16) | copy-start | bytes 393220
  49.9 52.9 %copy-start.1 = (bf16[16,128,256]{2,1,0:T(8,128)(2,1)}, bf16[16,128,256]{2,1,0:T(8,128)(2,1)S(1)}, u32[]{:S(2)}) copy-start(bf16[16,128,256]{2,1,0:T(8,128)(2,1)S(1)} %all-to-all-done.1) | copy-start | bytes 3145732
  102.8 3.9 %copy-start.2 = (bf16[2048,256]{1,0:T(8,128)(2,1)S(1)}, bf16[2048,256]{1,0:T(8,128)(2,1)}, u32[]{:S(2)}) copy-start(bf16[2048,256]{1,0:T(8,128)(2,1)} %param.31) | copy-start | bytes 3145732
  102.8 33.5 %all-to-all-start.2 = ((bf16[16,128,512]{2,1,0:T(8,128)(2,1)}), bf16[16,128,512]{2,1,0:T(8,128)(2,1)S(1)}, u32[]{:S(2)}, u32[]{:S(2)}) async-start(bf16[16,128,512]{2,1,0:T(8,128)(2,1)} %broadcast_in_dim.31), calls=%async_computation.2 | async-start | bytes 4194304 | tf_op jit(solution)/shard_map/all_to_all | solution.py:260
  136.3 1.4 copy-start
  137.6 52.6 %all-to-all-start.4 = ((bf16[8,512,256]{2,1,0:T(8,128)(2,1)}), bf16[8,512,256]{2,1,0:T(8,128)(2,1)}, u32[]{:S(2)}, u32[]{:S(2)}) async-start(bf16[8,512,256]{2,1,0:T(8,128)(2,1)} %pad_maximum_fusion.1), calls=%async_computation.4 | async-start | bytes 4194304 | tf_op jit(solution)/shard_map/all_to_all | solution.py:260
  228.3 1.0 copy-start.4
where the time goes:
time: 231 us; the launch traced here: 230 us
  blocking collectives  97.6 us (42%)
  waiting for transfers between devices  83.9 us (36%)
  Pallas kernels  26.9 us (12%)
  starting transfers between devices  11.8 us (5%)
  local copies, waits for them, and re-layouts  6.39 us (3%)
  other arithmetic  3.25 us (1%)
    all_to_all x3, blocking collectives, exchange(): return lax.all_to_all(x, axes, split_axis=0, concat_axis=0, tiled=True)  97.6 us
    all_to_all x3, waiting for transfers between devices, exchange(): return lax.all_to_all(x, axes, split_axis=0, concat_axis=0, tiled=True)  83.9 us
    all_to_all x3, starting transfers between devices, exchange(): return lax.all_to_all(x, axes, split_axis=0, concat_axis=0, tiled=True)  11.8 us
    pallas_call x1, Pallas kernels, on_device(): pl.pallas_call(project_kernel, grid_spec=pltpu.PrefetchScalarGridSpec(num...  8.24 us
    pallas_call x1, Pallas kernels, on_device(): pl.pallas_call(feed_kernel, grid=(inner,), in_specs=[pl.BlockSpec((tokens...  7.09 us
    pallas_call x1, Pallas kernels, on_device(): pl.pallas_call(scan_kernel, grid_spec=pltpu.PrefetchScalarGridSpec(num_sc...  6.72 us
    pallas_call x1, Pallas kernels, on_device(): pl.pallas_call(settle_kernel, grid_spec=pltpu.PrefetchScalarGridSpec(num_...  4.88 us
  transfers between devices with their start and end apart: 3, of which 3 were waited for; matrix products, arithmetic and copies ran while one was open for 1% of the time, Pallas kernels for 4%

commit v1 on v0

--- a/solution.py
+++ b/solution.py
@@ -5,6 +5,7 @@
 from jax.experimental.pallas import tpu as pltpu
 from jax.sharding import Mesh
 from jax.sharding import PartitionSpec as P
+
 
 CHAN = 16
 NORM_W = 128
@@ -15,6 +16,8 @@
 SIN = (3.1415926532428884, -5.167712741152494, 2.5501627931734125, -0.5992473907509345, 0.08203117351788075, -0.00700041798679132)
 COS = (0.9999999997799042, -4.934802137078826, 4.058709159556303, -1.33521200305024, 0.23493731381503577, -0.02439632434807213)
 FADE = (1.0, -1.0 / 2, 1.0 / 6, -1.0 / 24, 1.0 / 120, -1.0 / 720, 1.0 / 5040, -1.0 / 40320)
+CORES = 2
+EVERY = ("zh", "q", "y", "c")
 F32 = jnp.float32
 BF16 = jnp.bfloat16
 
@@ -101,7 +104,7 @@
     rank_ref, input_ref, pace_ref, surge_ref, long_rate_ref, short_rate_ref, long_turn_ref, short_turn_ref,
     long_maps_ref, short_maps_ref, maps_ref, ends_ref, tail_ref,
 ):
-    tokens, width = input_ref.shape
+    tokens, _ = input_ref.shape
     groups = pace_ref.shape[0]
     _, pairs, long_states = long_rate_ref.shape
     short_states = short_rate_ref.shape[2]
@@ -162,16 +165,20 @@
                 p_re * e_im + p_im * e_re + s_im,
             ]
         for i in range(4):
-            ends_ref[4 * d + i : 4 * d + i + 1, :] = total[i]
+            ends_ref[0, 4 * d + i : 4 * d + i + 1, :] = total[i]
+    for s in range(1, ends_ref.shape[0]):
+        ends_ref[s] = ends_ref[0]
 
 
 def settle_kernel(
-    place_ref, maps_ref, ends_ref, input_ref, skip_ref, gain_ref, long_maps_ref, short_maps_ref, merged_ref, carry_ref
+    place_ref, maps_ref, ends_ref, input_ref, skip_ref, gain_ref, long_maps_ref, short_maps_ref, residual_ref,
+    rows_ref, carry_ref,
 ):
     tokens, width = input_ref.shape
     lanes = maps_ref.shape[3]
     steps = tokens // CHUNKS
     members = ends_ref.shape[0]
+    rows = rows_ref.shape[1]
     me = place_ref[1]
     total = jnp.zeros((tokens, width), F32)
     for d in range(2):
@@ -219,49 +226,96 @@
         block = slice(at, at + NORM_W)
         part = active[:, block]
         part = part * lax.rsqrt(jnp.mean(part * part, axis=1, keepdims=True) + EPSILON)
-        merged_ref[:, block] = (part * gain_ref[:, block]).astype(BF16)
-
-
-def project_kernel(place_ref, merged_ref, residual_ref, emit_ref, gain_ref, normed_ref, own_ref):
-    _, members, tokens, width = merged_ref.shape
-    features = residual_ref.shape[3]
-    depth = members * features
-    projected = jnp.zeros((tokens, depth), F32)
+        part = (part * gain_ref[:, block]).astype(BF16)
+        for t in range(rows_ref.shape[0]):
+            rows_ref[t, :, block] = part[t * rows : (t + 1) * rows]
+    for t in range(rows_ref.shape[0]):
+        rows_ref[t, :, width:] = residual_ref[t * rows : (t + 1) * rows, :]
+
+
+def project_kernel(rows_ref, emit_ref, gain_ref, normed_ref, middle_ref):
+    members, features = middle_ref.shape[0], middle_ref.shape[2]
+    width = rows_ref.shape[2] - features
+    middle = jnp.concatenate([rows_ref[t, :, width:].astype(F32) for t in range(members)], axis=1)
     for t in range(members):
-        projected += jnp.dot(
-            merged_ref[0, t], emit_ref[t * width : (t + 1) * width, :], preferred_element_type=F32
+        middle += jnp.dot(
+            rows_ref[t, :, :width], emit_ref[t * width : (t + 1) * width, :], preferred_element_type=F32
         )
-    middle = projected + jnp.concatenate(
-        [residual_ref[0, t].astype(F32) for t in range(members)], axis=1
-    )
     scale = lax.rsqrt(jnp.mean(middle * middle, axis=1, keepdims=True) + EPSILON)
-    normed_ref[...] = (middle * scale * gain_ref[...]).astype(BF16)
+    normed = (middle * scale * gain_ref[...]).astype(BF16)
     for t in range(members):
-
-        @pl.when((place_ref[0] == t) & (place_ref[2] == pl.program_id(0)))
-        def _(t=t):
-            own_ref[...] = middle[:, t * features : (t + 1) * features]
-
-
-def feed_kernel(normed_ref, raise_ref, lower_ref, out_ref):
-    members, features = out_ref.shape[1], out_ref.shape[3]
-    upward = jnp.dot(normed_ref[...], raise_ref[...], preferred_element_type=F32)
+        middle_ref[t] = middle[:, t * features : (t + 1) * features]
+    for i in range(normed_ref.shape[0]):
+        for t in range(i % CORES, members, CORES):
+            at = t // CORES * features
+            normed_ref[i, :, at : at + features] = normed[:, t * features : (t + 1) * features]
+
+
+def up_kernel(start_ref, normed_ref, *refs):
+    *piece_refs, own_ref, sent_ref = refs
+    blocks = len(piece_refs) // CORES
+    deep, share = piece_refs[0].shape
+    for j in range(CORES):
+        total = 0.0
+        for m in range(blocks):
+            start = pl.multiple_of(start_ref[m], LANES) if blocks > 1 else 0
+            total += jnp.dot(
+                normed_ref[:, pl.ds(start, deep)], piece_refs[m * CORES + j][...], preferred_element_type=F32
+            )
+        own_ref[:, j * share : (j + 1) * share] = total
+        sent_ref[:, j * share : (j + 1) * share] = total.astype(BF16)
+
+
+def down_kernel(start_ref, own_ref, other_ref, *refs):
+    *piece_refs, out_ref, total_ref = refs
+    blocks = len(piece_refs) // CORES
+    share, deep = piece_refs[0].shape
+    parts, features = out_ref.shape[1], out_ref.shape[3]
+    upward = own_ref[...] + other_ref[...].astype(F32)
     hidden = jnp.square(jnp.maximum(upward, 0.0)).astype(BF16)
-    parts = [
-        jnp.dot(hidden, lower_ref[s], preferred_element_type=F32).astype(BF16)
-        for s in range(lower_ref.shape[0])
-    ]
-    whole = jnp.concatenate(parts, axis=1) if len(parts) > 1 else parts[0]
-    for t in range(members):
-        out_ref[0, t] = whole[:, t * features : (t + 1) * features]
+    for m in range(blocks):
+        start = pl.multiple_of(start_ref[m], LANES) if blocks > 1 else 0
+        total_ref[:, pl.ds(start, deep)] = sum(
+            jnp.dot(
+                hidden[:, j * share : (j + 1) * share], piece_refs[m * CORES + j][...], preferred_element_type=F32
+            )
+            for j in range(CORES)
+        )
+    for y in range(parts):
+        out_ref[0, y] = total_ref[:, y * features : (y + 1) * features].astype(BF16)
+
+
+def without_bit(x, bit):
+    return (x >> (bit + 1) << bit) | (x & ((1 << bit) - 1))
+
+
+def with_bit(x, bit, value):
+    return (x & ~(1 << bit)) | (value << bit)
+
+
+def routes(line, rows_y):
+    bit = (line // (rows_y * CORES)).bit_length() - 1
+    found = {}
+    for m in range(line):
+        if m >> bit & 1:
+            continue
+        for j in range(CORES):
+            pairs = []
+            for s in range(line):
+                for y in range(rows_y):
+                    for c in range(CORES):
+                        d = with_bit(s ^ m, bit, j ^ c)
+                        pairs.append(((s * rows_y + y) * CORES + c, (d * rows_y + y) * CORES + (s >> bit & 1)))
+            found[m, j] = pairs
+    return bit, found
 
 
 def exchange(x, axes):
     return lax.all_to_all(x, axes, split_axis=0, concat_axis=0, tiled=True)
 
 
-def everywhere(x, axes, members):
-    return exchange(jnp.broadcast_to(x[None], (members,) + x.shape), axes)
+def kernel(body, **more):
+    return pl.pallas_call(body, **more)
 
 
 def params(**more):
@@ -273,13 +327,14 @@
     paired_twist, unpaired_twist, paired_latent_linears, unpaired_latent_linears, skip_coefficient,
     closing_norm_multiplier, emitted_linear, leading_norm_multiplier, raising_linear, lowering_linear,
 ):
-    members = lax.axis_size("tp")
+    rows_y = lax.axis_size("y")
+    members = rows_y * CORES
     inner = lax.axis_size("q")
     line = HALVES * inner
-    rank = lax.axis_index("tp")
-    my_q = lax.axis_index("q")
-    me = lax.axis_index("zh") * inner + my_q
-    place = jnp.stack([rank, me, my_q]).astype(jnp.int32)
+    core = lax.axis_index("c")
+    rank = lax.axis_index("y") * CORES + core
+    me = lax.axis_index("zh") * inner + lax.axis_index("q")
+    place = jnp.stack([rank, me]).astype(jnp.int32)
     tokens, width = lifted_signal.shape
     groups = discrete_timestep.shape[0]
     pairs = groups // 2
@@ -287,20 +342,28 @@
     lanes = pairs * (long_states + short_states)
     depth_rows, hidden_columns = raising_linear.shape
     depth = depth_rows * line
+    half_depth = depth // CORES
     features = residual_signal.shape[1]
     share = hidden_columns // inner
-
-    raise_parts = raising_linear.reshape(depth_rows, inner, share).transpose(1, 0, 2)
-    raise_parts = jnp.concatenate([raise_parts] * HALVES, axis=0)
-    lower_parts = lowering_linear.reshape(inner, share, depth_rows)
-    lower_parts = jnp.concatenate([lower_parts] * HALVES, axis=0)
-    raised = exchange(raise_parts, ("zh", "q")).reshape(depth, share)
-    lowered = exchange(lower_parts, ("zh", "q"))
+    rows = tokens // members
+
+    bit, found = routes(line, rows_y)
+    up_pieces, down_pieces = [], []
+    for (m, j), pairs_of in found.items():
+        start = with_bit(me ^ m, bit, j ^ core) % inner * share
+        up = lax.dynamic_slice_in_dim(raising_linear, start, share, 1)
+        down = lax.dynamic_slice_in_dim(lowering_linear, start, share, 0)
+        for piece, pieces in ((up, up_pieces), (down, down_pieces)):
+            pieces.append(lax.ppermute(piece, EVERY, pairs_of))
+    blocks = len(up_pieces) // CORES
+    order = without_bit(me, bit) ^ jnp.arange(blocks)
+    starts = (order * depth_rows).astype(jnp.int32)
     if depth_rows % LANES:
-        lowered = lowered.transpose(1, 0, 2).reshape(1, share, depth)
-    residual_all = everywhere(residual_signal, ("q", "tp"), inner * members).reshape(
-        inner, members, tokens, features
-    )
+        up_pieces = [jnp.stack(up_pieces[j::CORES])[order].reshape(half_depth, share) for j in range(CORES)]
+        down_pieces = [
+            jnp.stack(down_pieces[j::CORES])[order].transpose(1, 0, 2).reshape(share, half_depth)
+            for j in range(CORES)
+        ]
 
     long_maps = jnp.swapaxes(paired_latent_linears, 4, 5)
     short_maps = jnp.swapaxes(unpaired_latent_linears, 4, 5)
@@ -319,7 +382,7 @@
 
     long_spec = owned(2, 2, 2, pairs, CHAN, long_states, at=3)
     short_spec = owned(2, 2, 2, pairs, CHAN, short_states, at=3)
-    maps, ends = pl.pallas_call(
+    maps, ends = kernel(
         scan_kernel,
         grid_spec=pltpu.PrefetchScalarGridSpec(
             num_scalar_prefetch=1,
@@ -335,21 +398,20 @@
                 long_spec,
                 short_spec,
             ],
-            out_specs=[full(2, 4, tokens, lanes), full(8, lanes)],
+            out_specs=[full(2, 4, tokens, lanes), full(line, 8, lanes)],
             scratch_shapes=[pltpu.VMEM((4, CHUNKS, lanes), F32)],
         ),
         out_shape=[
             jax.ShapeDtypeStruct((2, 4, tokens, lanes), F32),
-            jax.ShapeDtypeStruct((8, lanes), F32),
+            jax.ShapeDtypeStruct((line, 8, lanes), F32),
         ],
         compiler_params=params(),
-        name="scan",
     )(
         place, lifted_signal, discrete_timestep, additional_log_fading, by_rank(paired_fading),
         by_rank(unpaired_fading), by_rank(paired_twist), by_rank(unpaired_twist), long_maps, short_maps,
     )
-    all_ends = everywhere(ends, ("zh", "q"), line)
-    merged = pl.pallas_call(
+    all_ends = exchange(ends, ("zh", "q"))
+    mixed = kernel(
         settle_kernel,
         grid_spec=pltpu.PrefetchScalarGridSpec(
             num_scalar_prefetch=1,
@@ -362,65 +424,71 @@
                 owned(1, width, at=1),
                 long_spec,
                 short_spec,
+                full(tokens, features),
             ],
-            out_specs=full(tokens, width),
+            out_specs=full(members, rows, width + features),
             scratch_shapes=[pltpu.VMEM((2, CHUNKS, lanes), F32)],
         ),
-        out_shape=jax.ShapeDtypeStruct((tokens, width), BF16),
+        out_shape=jax.ShapeDtypeStruct((members, rows, width + features), BF16),
         compiler_params=params(),
-        name="settle",
     )(
         place, maps, all_ends, lifted_signal, skip_coefficient[None], closing_norm_multiplier[None],
-        long_maps, short_maps,
+        long_maps, short_maps, residual_signal,
     )
-    merged_all = everywhere(merged, ("q", "tp"), inner * members).reshape(inner, members, tokens, width)
-
-    normed, own = pl.pallas_call(
+    mixed_rows = exchange(mixed, ("y", "c"))
+    normed, middle = kernel(
         project_kernel,
+        out_shape=[
+            jax.ShapeDtypeStruct((inner * members, rows, half_depth), BF16),
+            jax.ShapeDtypeStruct((members, rows, features), F32),
+        ],
+        compiler_params=params(),
+    )(mixed_rows, emitted_linear, leading_norm_multiplier[None])
+    normed_all = exchange(normed, ("q", "y", "c")).reshape(inner * tokens, half_depth)
+    middle_own = exchange(middle, ("y", "c")).reshape(tokens, features)
+
+    def block(*shape):
+        return pl.BlockSpec(shape, lambda i, start_ref: (i,) + (0,) * (len(shape) - 1))
+
+    hidden_wide = CORES * share
+    own, sent = kernel(
+        up_kernel,
         grid_spec=pltpu.PrefetchScalarGridSpec(
             num_scalar_prefetch=1,
             grid=(inner,),
-            in_specs=[
-                pl.BlockSpec((1, members, tokens, width), lambda i, place_ref: (i, 0, 0, 0)),
-                pl.BlockSpec((1, members, tokens, features), lambda i, place_ref: (i, 0, 0, 0)),
-                full(members * width, depth),
-                full(1, depth),
-            ],
-            out_specs=[
-                pl.BlockSpec((tokens, depth), lambda i, place_ref: (i, 0)),
-                full(tokens, features),
-            ],
+            in_specs=[block(tokens, half_depth)] + [full(*piece.shape) for piece in up_pieces],
+            out_specs=[block(tokens, hidden_wide), block(tokens, hidden_wide)],
         ),
         out_shape=[
-            jax.ShapeDtypeStruct((inner * tokens, depth), BF16),
-            jax.ShapeDtypeStruct((tokens, features), F32),
+            jax.ShapeDtypeStruct((inner * tokens, hidden_wide), F32),
+            jax.ShapeDtypeStruct((inner * tokens, hidden_wide), BF16),
         ],
         compiler_params=params(),
-        name="project",
-    )(place, merged_all, residual_all, emitted_linear, leading_norm_multiplier[None])
-
-    partial = pl.pallas_call(
-        feed_kernel,
-        grid=(inner,),
-        in_specs=[
-            pl.BlockSpec((tokens, depth), lambda i: (i, 0)),
-            pl.BlockSpec((depth, share), lambda i: (0, 0)),
-            pl.BlockSpec(lowered.shape, lambda i: (0, 0, 0)),
-        ],
-        out_specs=pl.BlockSpec((1, members, tokens, features), lambda i: (i, 0, 0, 0)),
-        out_shape=jax.ShapeDtypeStruct((inner, members, tokens, features), BF16),
+    )(starts, normed_all, *up_pieces)
+    other = lax.ppermute(sent, "c", [(c, CORES - 1 - c) for c in range(CORES)])
+    partial = kernel(
+        down_kernel,
+        grid_spec=pltpu.PrefetchScalarGridSpec(
+            num_scalar_prefetch=1,
+            grid=(inner,),
+            in_specs=[block(tokens, hidden_wide), block(tokens, hidden_wide)]
+            + [full(*piece.shape) for piece in down_pieces],
+            out_specs=block(1, rows_y, tokens, features),
+            scratch_shapes=[pltpu.VMEM((tokens, half_depth), F32)],
+        ),
+        out_shape=jax.ShapeDtypeStruct((inner, rows_y, tokens, features), BF16),
         compiler_params=params(),
-        name="feed",
-    )(normed, raised, lowered)
-    shares = exchange(partial.reshape(inner * members, tokens, features), ("q", "tp"))
-    return (own + jnp.sum(shares.astype(F32), axis=0)).astype(BF16)
+    )(starts, own, other, *down_pieces)
+    shares = exchange(partial.reshape(inner * rows_y, tokens, features), ("q", "y"))
+    return (middle_own + jnp.sum(shares.astype(F32), axis=0)).astype(BF16)
 
 
 def solution(mesh):
     sp, tp = mesh.axis_names
     line, members = mesh.shape[sp], mesh.shape[tp]
-    split = Mesh(mesh.devices.reshape(HALVES, line // HALVES, members), ("zh", "q", "tp"))
-    s, t = ("zh", "q"), "tp"
+    rows_y = members // CORES
+    split = Mesh(mesh.devices.reshape(HALVES, line // HALVES, rows_y, CORES), EVERY)
+    s, t = EVERY[:2], EVERY[2:]
     in_specs = (P(s, t), P(s, t), P(t, s), P(t, s)) + (P(),) * 10 + (P(s, t), P(t, s))
     return jax.shard_map(
         on_device, mesh=split, in_specs=in_specs, out_specs=P(s, t), check_vma=False

time: 231 us -> 201 us (0.87)
  blocking collectives: 97.6 us -> 43.3 us
  starting transfers between devices: 11.8 us -> 56.2 us
  waiting for transfers between devices: 83.9 us -> 67.5 us
  local copies, waits for them, and re-layouts: 6.39 us -> 3.24 us
    all_to_all x3 -> x2, waiting for transfers between devices: 83.9 us -> 5.83 us  [exchange(): return lax.all_to_all(x, axes, split_axis=0, concat_axis=0, tiled=True)]
    ppermute x0 -> x17, waiting for transfers between devices: none -> 61.7 us  [the longest x16 61.7 us: on_device(): pieces.append(lax.ppermute(piece, EVERY, pairs_of))]
    all_to_all x3, blocking collectives: 97.6 us -> 43.3 us  [exchange(): return lax.all_to_all(x, axes, split_axis=0, concat_axis=0, tiled=True)]
    ppermute x0 -> x17, starting transfers between devices: none -> 49 us  [the longest x16 49 us: on_device(): pieces.append(lax.ppermute(piece, EVERY, pairs_of))]
    all_to_all x3 -> x2, starting transfers between devices: 11.8 us -> 7.19 us  [exchange(): return lax.all_to_all(x, axes, split_axis=0, concat_axis=0, tiled=True)]
    broadcast_in_dim x3 -> x0, local copies, waits for them, and re-layouts: 4.27 us -> none  [everywhere(): return exchange(jnp.broadcast_to(x[None], (members,) + x.shape), axes)]
    pallas_call x4 -> x5, Pallas kernels: 26.9 us -> 27.9 us  [the longest x1 6.78 us: on_device(): kernel(scan_kernel, grid_spec=pltpu.PrefetchScalarGridSpec(num_scalar_pre...]
  transfers between devices with their start and end apart: 3 -> 19, of which waited for: 3 -> 7; matrix products, arithmetic and copies ran while one was open for 1% -> 1% of each run, Pallas kernels for 4% -> 0%
where the time goes in v1:
time: 201 us; the launch traced here: 200 us
  waiting for transfers between devices  67.5 us (34%)
  starting transfers between devices  56.2 us (28%)
  blocking collectives  43.3 us (22%)
  Pallas kernels  27.9 us (14%)
  local copies, waits for them, and re-layouts  3.24 us (2%)
    ppermute x16, waiting for transfers between devices, on_device(): pieces.append(lax.ppermute(piece, EVERY, pairs_of))  61.7 us
    ppermute x16, starting transfers between devices, on_device(): pieces.append(lax.ppermute(piece, EVERY, pairs_of))  49 us
    all_to_all x3, blocking collectives, exchange(): return lax.all_to_all(x, axes, split_axis=0, concat_axis=0, tiled=True)  43.3 us
    all_to_all x2, starting transfers between devices, exchange(): return lax.all_to_all(x, axes, split_axis=0, concat_axis=0, tiled=True)  7.19 us
    pallas_call x1, Pallas kernels, on_device(): kernel(scan_kernel, grid_spec=pltpu.PrefetchScalarGridSpec(num_scalar_pre...  6.78 us
    pallas_call x1, Pallas kernels, on_device(): kernel(up_kernel, grid_spec=pltpu.PrefetchScalarGridSpec(num_scalar_prefe...  5.99 us
    pallas_call x1, Pallas kernels, on_device(): kernel(down_kernel, grid_spec=pltpu.PrefetchScalarGridSpec(num_scalar_pre...  5.98 us
    all_to_all x2, waiting for transfers between devices, exchange(): return lax.all_to_all(x, axes, split_axis=0, concat_axis=0, tiled=True)  5.83 us
  transfers between devices with their start and end apart: 19, of which 7 were waited for; matrix products, arithmetic and copies ran while one was open for 1% of the time, Pallas kernels for 0%

profile of v1, /device:TPU:0, one launch (start us, length us, event | category | flops | bytes accessed | tf_op | source)
XLA Modules:
  0.0 200.4 jit_solution(12968141376609344641)
XLA Ops:
  0.0 0.6 pad_add_fusion.rank_ref.place_ref
  0.6 6.8 %shard_map.154 = (f32[2,4,128,768]{3,2,1,0:T(8,128)}, f32[8,8,768]{2,1,0:T(8,128)}) custom-call(s32[2]{0:T(128)} %pad_add_fusion.rank_ref.place_ref, bf16[128,256]{1,0:T(8,128)(2,1)} %input_ref.3, f32[16,128]{1,0:T(8,128)} %pace_ref.1, f32[16,128]{1,0:T(8,128)} %surge_ref.1, f32[2,4,8,64]{3,2,1,0:T(8,128)} %bitcast.23, f32[2,4,8,32]{3,2,1,0:T(8,128)} %bitcast.24, ...), custom_call_target="tpu_custom_call" | custom-call | tf_op jit(solution)/shard_map/pallas_call | solution.py:385
  7.4 15.3 %all_to_all.25.ends_ref = f32[8,8,768]{2,1,0:T(8,128)} all-to-all(f32[8,8,768]{2,1,0:T(8,128)} %get-tuple-element.12), channel_id=1, replica_groups=mesh['zh'=2,'q'=4,'y'=2,'c'=2] {'zh','q'}, dimensions={0} | all-to-all | bytes 393216 | tf_op jit(solution)/shard_map/all_to_all | solution.py:314
  22.7 5.0 %shard_map.155 = bf16[4,32,768]{2,1,0:T(8,128)(2,1)} custom-call(s32[2]{0:T(128)} %pad_add_fusion.rank_ref.place_ref, f32[2,4,128,768]{3,2,1,0:T(8,128)} %get-tuple-element.11.maps_ref, f32[8,8,768]{2,1,0:T(8,128)} %all_to_all.25.ends_ref, bf16[128,256]{1,0:T(8,128)(2,1)} %input_ref.3, f32[1,1024]{1,0:T(1,128)} %bitcast.28, f32[1,1024]{1,0:T(1,128)} %bitcast.29, ...), custom_call_target="tpu_custom_call" | custom-call | tf_op jit(solution)/shard_map/pallas_call | solution.py:414
  27.7 9.3 %all_to_all.26.rows_ref = bf16[4,32,768]{2,1,0:T(8,128)(2,1)} all-to-all(bf16[4,32,768]{2,1,0:T(8,128)(2,1)} %shard_map.155), channel_id=1, replica_groups=mesh['zh'=2,'q'=4,'y'=2,'c'=2] {'y','c'}, dimensions={0} | all-to-all | bytes 393216 | tf_op jit(solution)/shard_map/all_to_all | solution.py:314
  37.0 4.1 %shard_map.156 = (bf16[16,32,1024]{2,1,0:T(8,128)(2,1)}, f32[4,32,512]{2,1,0:T(8,128)}) custom-call(bf16[4,32,768]{2,1,0:T(8,128)(2,1)} %all_to_all.26.rows_ref, bf16[1024,2048]{1,0:T(8,128)(2,1)} %emit_ref.1, f32[1,2048]{1,0:T(1,128)} %bitcast.27), custom_call_target="tpu_custom_call" | custom-call | tf_op jit(solution)/shard_map/pallas_call | solution.py:439
  41.2 3.8 %all-to-all-start.3 = ((bf16[16,32,1024]{2,1,0:T(8,128)(2,1)}), bf16[16,32,1024]{2,1,0:T(8,128)(2,1)S(1)}, u32[]{:S(2)}, u32[]{:S(2)}) async-start(bf16[16,32,1024]{2,1,0:T(8,128)(2,1)} %get-tuple-element.14), calls=%async_computation.3 | async-start | bytes 2097152 | tf_op jit(solution)/shard_map/all_to_all | solution.py:314
  45.1 0.3 constant_dynamic-slice_fusion.8
  45.4 0.0 copy-start.1
  45.4 0.8 collective-permute-start
  46.2 3.0 %collective-permute-start.1 = (bf16[256,512]{1,0:T(8,128)(2,1)S(1)}, bf16[256,512]{1,0:T(8,128)(2,1)S(1)}, u32[]{:S(2)}, u32[]{:S(2)}) collective-permute-start(bf16[256,512]{1,0:T(8,128)(2,1)S(1)} %get-tuple-element.30), channel_id=1, source_target_pairs={{0,8},{1,0},{2,10},{3,2},{4,12},{5,4},{6,14},{7,6},{8,9},{9,1},{10... | collective-permute-start | bytes 786440 | tf_op jit(solution)/shard_map/ppermute | solution.py:357
  49.3 1.7 collective-permute-start.2
  50.9 1.0 collective-permute-start.3
  51.9 0.7 collective-permute-start.4
  52.6 15.3 %collective-permute-start.5 = (bf16[256,512]{1,0:T(8,128)(2,1)S(1)}, bf16[256,512]{1,0:T(8,128)(2,1)}, u32[]{:S(2)}, u32[]{:S(2)}) collective-permute-start(bf16[256,512]{1,0:T(8,128)(2,1)S(1)} %get-tuple-element.26), channel_id=1, source_target_pairs={{0,24},{1,16},{2,26},{3,18},{4,28},{5,20},{6,30},{7,22},{8,25},{9,... | collective-permute-start | bytes 786440 | tf_op jit(solution)/shard_map/ppermute | solution.py:357
  67.9 0.0 collective-permute-done.1.refs_1_
  67.9 5.1 %collective-permute-start.6 = (bf16[256,512]{1,0:T(8,128)(2,1)S(1)}, bf16[256,512]{1,0:T(8,128)(2,1)}, u32[]{:S(2)}, u32[]{:S(2)}) collective-permute-start(bf16[256,512]{1,0:T(8,128)(2,1)S(1)} %get-tuple-element.32), channel_id=1, source_target_pairs={{0,20},{1,28},{2,22},{3,30},{4,16},{5,24},{6,18},{7,26},{8,21},{9,... | collective-permute-start | bytes 786440 | tf_op jit(solution)/shard_map/ppermute | solution.py:357
  73.0 0.0 collective-permute-done.2.refs_2_
  73.1 0.7 copy-done.14
  73.8 2.5 %collective-permute-start.7 = (bf16[256,512]{1,0:T(8,128)(2,1)S(1)}, bf16[256,512]{1,0:T(8,128)(2,1)}, u32[]{:S(2)}, u32[]{:S(2)}) collective-permute-start(bf16[256,512]{1,0:T(8,128)(2,1)S(1)} %get-tuple-element.25), channel_id=1, source_target_pairs={{0,28},{1,20},{2,30},{3,22},{4,24},{5,16},{6,26},{7,18},{8,29},{9,... | collective-permute-start | bytes 786440 | tf_op jit(solution)/shard_map/ppermute | solution.py:357
  76.2 0.5 xor_multiply_fusion.start_ref
  76.8 0.0 collective-permute-done.3.refs_3_
  76.8 0.0 collective-permute-done.4.refs_4_
  76.8 3.3 %collective-permute-done.5.refs_5_ = bf16[256,512]{1,0:T(8,128)(2,1)} collective-permute-done((bf16[256,512]{1,0:T(8,128)(2,1)S(1)}, bf16[256,512]{1,0:T(8,128)(2,1)}, u32[]{:S(2)}, u32[]{:S(2)}) %collective-permute-start.5) | collective-permute-done | bytes 262176 | tf_op jit(solution)/shard_map/ppermute | solution.py:357
  80.0 25.4 %collective-permute-done.6.refs_6_ = bf16[256,512]{1,0:T(8,128)(2,1)} collective-permute-done((bf16[256,512]{1,0:T(8,128)(2,1)S(1)}, bf16[256,512]{1,0:T(8,128)(2,1)}, u32[]{:S(2)}, u32[]{:S(2)}) %collective-permute-start.6) | collective-permute-done | bytes 262176 | tf_op jit(solution)/shard_map/ppermute | solution.py:357
  105.4 1.0 copy-done.2
  106.4 6.0 %shard_map.157 = (f32[512,1024]{1,0:T(8,128)}, bf16[512,1024]{1,0:T(8,128)(2,1)}) custom-call(s32[4]{0:T(128)} %xor_multiply_fusion.start_ref, bf16[512,1024]{1,0:T(8,128)(2,1)} %bitcast.22, bf16[256,512]{1,0:T(8,128)(2,1)} %copy-done.12, bf16[256,512]{1,0:T(8,128)(2,1)} %copy-done.13, bf16[256,512]{1,0:T(8,128)(2,1)} %copy-done.14, ...), custom_call_target="tpu_custom_call" | custom-call | tf_op jit(solution)/shard_map/pallas_call | solution.py:454
  112.4 0.2 constant_dynamic-slice_fusion
  112.6 3.4 %collective-permute-start.10 = (bf16[512,256]{1,0:T(8,128)(2,1)S(1)}, bf16[512,256]{1,0:T(8,128)(2,1)S(1)}, u32[]{:S(2)}, u32[]{:S(2)}) collective-permute-start(bf16[512,256]{1,0:T(8,128)(2,1)S(1)} %get-tuple-element.22), channel_id=1, source_target_pairs={{0,8},{1,0},{2,10},{3,2},{4,12},{5,4},{6,14},{7,6},{8,9},{9,1},{10... | collective-permute-start | bytes 786440 | tf_op jit(solution)/shard_map/ppermute | solution.py:357
  116.0 0.5 collective-permute-start.11
  116.6 1.8 collective-permute-start.13
  118.4 4.4 %collective-permute-done.10.refs_1_ = bf16[512,256]{1,0:T(8,128)(2,1)S(1)} collective-permute-done((bf16[512,256]{1,0:T(8,128)(2,1)S(1)}, bf16[512,256]{1,0:T(8,128)(2,1)S(1)}, u32[]{:S(2)}, u32[]{:S(2)}) %collective-permute-start.10) | collective-permute-done | bytes 262176 | tf_op jit(solution)/shard_map/ppermute | solution.py:357
  122.7 7.6 %collective-permute-start.14 = (bf16[512,256]{1,0:T(8,128)(2,1)S(1)}, bf16[512,256]{1,0:T(8,128)(2,1)S(1)}, u32[]{:S(2)}, u32[]{:S(2)}) collective-permute-start(bf16[512,256]{1,0:T(8,128)(2,1)S(1)} %get-tuple-element.18), channel_id=1, source_target_pairs={{0,24},{1,16},{2,26},{3,18},{4,28},{5,20},{6,30},{7,22},{8,25},{9,... | collective-permute-start | bytes 786440 | tf_op jit(solution)/shard_map/ppermute | solution.py:357
  130.4 1.3 collective-permute-start.15
  131.7 3.6 %collective-permute-start.16 = (bf16[512,256]{1,0:T(8,128)(2,1)S(1)}, bf16[512,256]{1,0:T(8,128)(2,1)S(1)}, u32[]{:S(2)}, u32[]{:S(2)}) collective-permute-start(bf16[512,256]{1,0:T(8,128)(2,1)S(1)} %get-tuple-element.17), channel_id=1, source_target_pairs={{0,28},{1,20},{2,30},{3,22},{4,24},{5,16},{6,26},{7,18},{8,29},{9,... | collective-permute-start | bytes 786440 | tf_op jit(solution)/shard_map/ppermute | solution.py:357
  135.3 0.7 collective-permute-start.9
  135.9 18.5 %collective-permute-done.14.refs_5_ = bf16[512,256]{1,0:T(8,128)(2,1)S(1)} collective-permute-done((bf16[512,256]{1,0:T(8,128)(2,1)S(1)}, bf16[512,256]{1,0:T(8,128)(2,1)S(1)}, u32[]{:S(2)}, u32[]{:S(2)}) %collective-permute-start.14) | collective-permute-done | bytes 262176 | tf_op jit(solution)/shard_map/ppermute | solution.py:357
  154.4 6.9 %collective-permute-done.15.refs_6_ = bf16[512,256]{1,0:T(8,128)(2,1)S(1)} collective-permute-done((bf16[512,256]{1,0:T(8,128)(2,1)S(1)}, bf16[512,256]{1,0:T(8,128)(2,1)S(1)}, u32[]{:S(2)}, u32[]{:S(2)}) %collective-permute-start.15) | collective-permute-done | bytes 262176 | tf_op jit(solution)/shard_map/ppermute | solution.py:357
  161.3 3.3 %collective-permute-done.16.refs_7_ = bf16[512,256]{1,0:T(8,128)(2,1)S(1)} collective-permute-done((bf16[512,256]{1,0:T(8,128)(2,1)S(1)}, bf16[512,256]{1,0:T(8,128)(2,1)S(1)}, u32[]{:S(2)}, u32[]{:S(2)}) %collective-permute-start.16) | collective-permute-done | bytes 262176 | tf_op jit(solution)/shard_map/ppermute | solution.py:357
  164.7 0.6 copy-done.10
  165.3 0.1 copy-done.11
  165.4 0.3 copy-done.3
  165.7 6.0 %shard_map.158 = bf16[4,2,128,512]{3,2,1,0:T(8,128)(2,1)} custom-call(s32[4]{0:T(128)} %xor_multiply_fusion.start_ref, f32[512,1024]{1,0:T(8,128)} %get-tuple-element.15.own_ref, bf16[512,1024]{1,0:T(8,128)(2,1)} %copy-done.3, bf16[512,256]{1,0:T(8,128)(2,1)} %copy-done.11, bf16[512,256]{1,0:T(8,128)(2,1)} %copy-done.4, bf16[512,256]{1,0:T(8,128)(2,1)} %copy-done.5, ...), custom_call_target="tpu_custom_call" | custom-call | tf_op jit(solution)/shard_map/pallas_call | solution.py:469
  171.7 18.6 %all_to_all.27 = bf16[8,128,512]{2,1,0:T(8,128)(2,1)S(1)} all-to-all(bf16[8,128,512]{2,1,0:T(8,128)(2,1)} %bitcast.21), channel_id=1, replica_groups=mesh['zh'=2,'q'=4,'y'=2,'c'=2] {'q','y'}, dimensions={0} | all-to-all | bytes 2097152 | tf_op jit(solution)/shard_map/all_to_all | solution.py:314
  190.3 3.4 %all-to-all-start.2 = ((f32[4,32,512]{2,1,0:T(8,128)}), f32[4,32,512]{2,1,0:T(8,128)S(1)}, u32[]{:S(2)}, u32[]{:S(2)}) async-start(f32[4,32,512]{2,1,0:T(8,128)} %get-tuple-element.13), calls=%async_computation.2 | async-start | bytes 524288 | tf_op jit(solution)/shard_map/all_to_all | solution.py:314
  193.7 0.1 convert_reduce_fusion
  193.9 5.8 %all-to-all-done.2 = f32[4,32,512]{2,1,0:T(8,128)S(1)} async-done(((f32[4,32,512]{2,1,0:T(8,128)}), f32[4,32,512]{2,1,0:T(8,128)S(1)}, u32[]{:S(2)}, u32[]{:S(2)}) %all-to-all-start.2) | async-done | bytes 262176 | tf_op jit(solution)/shard_map/all_to_all | solution.py:314
  199.7 0.7 fusion
  (34 shorter events, 0.1 us)
Async XLA Ops:
  41.2 4.0 %copy-start = (bf16[256,2048]{1,0:T(8,128)(2,1)S(1)}, bf16[256,2048]{1,0:T(8,128)(2,1)}, u32[]{:S(2)}) copy-start(bf16[256,2048]{1,0:T(8,128)(2,1)} %param.30) | copy-start | bytes 3145732
  41.2 64.3 %all-to-all-start.3 = ((bf16[16,32,1024]{2,1,0:T(8,128)(2,1)}), bf16[16,32,1024]{2,1,0:T(8,128)(2,1)S(1)}, u32[]{:S(2)}, u32[]{:S(2)}) async-start(bf16[16,32,1024]{2,1,0:T(8,128)(2,1)} %get-tuple-element.14), calls=%async_computation.3 | async-start | bytes 2097152 | tf_op jit(solution)/shard_map/all_to_all | solution.py:314
  45.4 67.0 %copy-start.1 = (bf16[2048,256]{1,0:T(8,128)(2,1)S(1)}, bf16[2048,256]{1,0:T(8,128)(2,1)}, u32[]{:S(2)}) copy-start(bf16[2048,256]{1,0:T(8,128)(2,1)} %param.31) | copy-start | bytes 3145732
  45.4 7.2 %collective-permute-start = (bf16[256,512]{1,0:T(8,128)(2,1)S(1)}, bf16[256,512]{1,0:T(8,128)(2,1)S(1)}, u32[]{:S(2)}, u32[]{:S(2)}) collective-permute-start(bf16[256,512]{1,0:T(8,128)(2,1)S(1)} %get-tuple-element.31), channel_id=1, source_target_pairs={{0,0},{1,8},{2,2},{3,10},{4,4},{5,12},{6,6},{7,14},{8,1},{9,9},{10... | collective-permute-start | bytes 786440 | tf_op jit(solution)/shard_map/ppermute | solution.py:357
  46.2 21.7 %collective-permute-start.1 = (bf16[256,512]{1,0:T(8,128)(2,1)S(1)}, bf16[256,512]{1,0:T(8,128)(2,1)S(1)}, u32[]{:S(2)}, u32[]{:S(2)}) collective-permute-start(bf16[256,512]{1,0:T(8,128)(2,1)S(1)} %get-tuple-element.30), channel_id=1, source_target_pairs={{0,8},{1,0},{2,10},{3,2},{4,12},{5,4},{6,14},{7,6},{8,9},{9,1},{10... | collective-permute-start | bytes 786440 | tf_op jit(solution)/shard_map/ppermute | solution.py:357
  49.3 23.8 %collective-permute-start.2 = (bf16[256,512]{1,0:T(8,128)(2,1)S(1)}, bf16[256,512]{1,0:T(8,128)(2,1)S(1)}, u32[]{:S(2)}, u32[]{:S(2)}) collective-permute-start(bf16[256,512]{1,0:T(8,128)(2,1)S(1)} %get-tuple-element.29), channel_id=1, source_target_pairs={{0,4},{1,12},{2,6},{3,14},{4,0},{5,8},{6,2},{7,10},{8,5},{9,13},{1... | collective-permute-start | bytes 786440 | tf_op jit(solution)/shard_map/ppermute | solution.py:357
  50.9 25.8 %collective-permute-start.3 = (bf16[256,512]{1,0:T(8,128)(2,1)S(1)}, bf16[256,512]{1,0:T(8,128)(2,1)}, u32[]{:S(2)}, u32[]{:S(2)}) collective-permute-start(bf16[256,512]{1,0:T(8,128)(2,1)S(1)} %get-tuple-element.28), channel_id=1, source_target_pairs={{0,12},{1,4},{2,14},{3,6},{4,8},{5,0},{6,10},{7,2},{8,13},{9,5},{1... | collective-permute-start | bytes 786440 | tf_op jit(solution)/shard_map/ppermute | solution.py:357
  51.9 24.8 %collective-permute-start.4 = (bf16[256,512]{1,0:T(8,128)(2,1)S(1)}, bf16[256,512]{1,0:T(8,128)(2,1)}, u32[]{:S(2)}, u32[]{:S(2)}) collective-permute-start(bf16[256,512]{1,0:T(8,128)(2,1)S(1)} %get-tuple-element.27), channel_id=1, source_target_pairs={{0,16},{1,24},{2,18},{3,26},{4,20},{5,28},{6,22},{7,30},{8,17},{9,... | collective-permute-start | bytes 786440 | tf_op jit(solution)/shard_map/ppermute | solution.py:357
  52.6 20.4 %copy-start.12 = (bf16[256,512]{1,0:T(8,128)(2,1)}, bf16[256,512]{1,0:T(8,128)(2,1)S(1)}, u32[]{:S(2)}) copy-start(bf16[256,512]{1,0:T(8,128)(2,1)S(1)} %collective-permute-done.refs_0_) | copy-start | bytes 786436
  52.6 27.4 %collective-permute-start.5 = (bf16[256,512]{1,0:T(8,128)(2,1)S(1)}, bf16[256,512]{1,0:T(8,128)(2,1)}, u32[]{:S(2)}, u32[]{:S(2)}) collective-permute-start(bf16[256,512]{1,0:T(8,128)(2,1)S(1)} %get-tuple-element.26), channel_id=1, source_target_pairs={{0,24},{1,16},{2,26},{3,18},{4,28},{5,20},{6,30},{7,22},{8,25},{9,... | collective-permute-start | bytes 786440 | tf_op jit(solution)/shard_map/ppermute | solution.py:357
  67.9 5.1 %copy-start.13 = (bf16[256,512]{1,0:T(8,128)(2,1)}, bf16[256,512]{1,0:T(8,128)(2,1)S(1)}, u32[]{:S(2)}) copy-start(bf16[256,512]{1,0:T(8,128)(2,1)S(1)} %collective-permute-done.1.refs_1_) | copy-start | bytes 786436
  67.9 37.5 %collective-permute-start.6 = (bf16[256,512]{1,0:T(8,128)(2,1)S(1)}, bf16[256,512]{1,0:T(8,128)(2,1)}, u32[]{:S(2)}, u32[]{:S(2)}) collective-permute-start(bf16[256,512]{1,0:T(8,128)(2,1)S(1)} %get-tuple-element.32), channel_id=1, source_target_pairs={{0,20},{1,28},{2,22},{3,30},{4,16},{5,24},{6,18},{7,26},{8,21},{9,... | collective-permute-start | bytes 786440 | tf_op jit(solution)/shard_map/ppermute | solution.py:357
  73.0 0.7 copy-start.14
  73.8 31.7 %collective-permute-start.7 = (bf16[256,512]{1,0:T(8,128)(2,1)S(1)}, bf16[256,512]{1,0:T(8,128)(2,1)}, u32[]{:S(2)}, u32[]{:S(2)}) collective-permute-start(bf16[256,512]{1,0:T(8,128)(2,1)S(1)} %get-tuple-element.25), channel_id=1, source_target_pairs={{0,28},{1,20},{2,30},{3,22},{4,24},{5,16},{6,26},{7,18},{8,29},{9,... | collective-permute-start | bytes 786440 | tf_op jit(solution)/shard_map/ppermute | solution.py:357
  105.4 1.0 copy-start.2
  112.4 52.2 %collective-permute-start.8 = (bf16[512,1024]{1,0:T(8,128)(2,1)}, bf16[512,1024]{1,0:T(8,128)(2,1)S(1)}, u32[]{:S(2)}, u32[]{:S(2)}) collective-permute-start(bf16[512,1024]{1,0:T(8,128)(2,1)} %get-tuple-element.16), channel_id=1, source_target_pairs={{0,1},{1,0},{2,3},{3,2},{4,5},{5,4},{6,7},{7,6},{8,9},{9,8},{10,11... | collective-permute-start | bytes 3145736 | tf_op jit(solution)/shard_map/ppermute | solution.py:468
  112.6 10.1 %collective-permute-start.10 = (bf16[512,256]{1,0:T(8,128)(2,1)S(1)}, bf16[512,256]{1,0:T(8,128)(2,1)S(1)}, u32[]{:S(2)}, u32[]{:S(2)}) collective-permute-start(bf16[512,256]{1,0:T(8,128)(2,1)S(1)} %get-tuple-element.22), channel_id=1, source_target_pairs={{0,8},{1,0},{2,10},{3,2},{4,12},{5,4},{6,14},{7,6},{8,9},{9,1},{10... | collective-permute-start | bytes 786440 | tf_op jit(solution)/shard_map/ppermute | solution.py:357
  116.0 14.4 %collective-permute-start.11 = (bf16[512,256]{1,0:T(8,128)(2,1)S(1)}, bf16[512,256]{1,0:T(8,128)(2,1)S(1)}, u32[]{:S(2)}, u32[]{:S(2)}) collective-permute-start(bf16[512,256]{1,0:T(8,128)(2,1)S(1)} %get-tuple-element.21), channel_id=1, source_target_pairs={{0,4},{1,12},{2,6},{3,14},{4,0},{5,8},{6,2},{7,10},{8,5},{9,13},{1... | collective-permute-start | bytes 786440 | tf_op jit(solution)/shard_map/ppermute | solution.py:357
  116.6 15.1 %collective-permute-start.12 = (bf16[512,256]{1,0:T(8,128)(2,1)S(1)}, bf16[512,256]{1,0:T(8,128)(2,1)S(1)}, u32[]{:S(2)}, u32[]{:S(2)}) collective-permute-start(bf16[512,256]{1,0:T(8,128)(2,1)S(1)} %get-tuple-element.20), channel_id=1, source_target_pairs={{0,12},{1,4},{2,14},{3,6},{4,8},{5,0},{6,10},{7,2},{8,13},{9,5},{1... | collective-permute-start | bytes 786440 | tf_op jit(solution)/shard_map/ppermute | solution.py:357
  116.6 18.7 %collective-permute-start.13 = (bf16[512,256]{1,0:T(8,128)(2,1)S(1)}, bf16[512,256]{1,0:T(8,128)(2,1)S(1)}, u32[]{:S(2)}, u32[]{:S(2)}) collective-permute-start(bf16[512,256]{1,0:T(8,128)(2,1)S(1)} %get-tuple-element.19), channel_id=1, source_target_pairs={{0,16},{1,24},{2,18},{3,26},{4,20},{5,28},{6,22},{7,30},{8,17},{9,... | collective-permute-start | bytes 786440 | tf_op jit(solution)/shard_map/ppermute | solution.py:357
  122.7 41.9 %copy-start.4 = (bf16[512,256]{1,0:T(8,128)(2,1)}, bf16[512,256]{1,0:T(8,128)(2,1)S(1)}, u32[]{:S(2)}) copy-start(bf16[512,256]{1,0:T(8,128)(2,1)S(1)} %collective-permute-done.10.refs_1_) | copy-start | bytes 786436
  122.7 31.7 %collective-permute-start.14 = (bf16[512,256]{1,0:T(8,128)(2,1)S(1)}, bf16[512,256]{1,0:T(8,128)(2,1)S(1)}, u32[]{:S(2)}, u32[]{:S(2)}) collective-permute-start(bf16[512,256]{1,0:T(8,128)(2,1)S(1)} %get-tuple-element.18), channel_id=1, source_target_pairs={{0,24},{1,16},{2,26},{3,18},{4,28},{5,20},{6,30},{7,22},{8,25},{9,... | collective-permute-start | bytes 786440 | tf_op jit(solution)/shard_map/ppermute | solution.py:357
  130.4 34.2 %copy-start.5 = (bf16[512,256]{1,0:T(8,128)(2,1)}, bf16[512,256]{1,0:T(8,128)(2,1)S(1)}, u32[]{:S(2)}) copy-start(bf16[512,256]{1,0:T(8,128)(2,1)S(1)} %collective-permute-done.11.refs_2_) | copy-start | bytes 786436
  130.4 30.9 %collective-permute-start.15 = (bf16[512,256]{1,0:T(8,128)(2,1)S(1)}, bf16[512,256]{1,0:T(8,128)(2,1)S(1)}, u32[]{:S(2)}, u32[]{:S(2)}) collective-permute-start(bf16[512,256]{1,0:T(8,128)(2,1)S(1)} %get-tuple-element.24), channel_id=1, source_target_pairs={{0,20},{1,28},{2,22},{3,30},{4,16},{5,24},{6,18},{7,26},{8,21},{9,... | collective-permute-start | bytes 786440 | tf_op jit(solution)/shard_map/ppermute | solution.py:357
  131.7 33.0 %copy-start.6 = (bf16[512,256]{1,0:T(8,128)(2,1)}, bf16[512,256]{1,0:T(8,128)(2,1)S(1)}, u32[]{:S(2)}) copy-start(bf16[512,256]{1,0:T(8,128)(2,1)S(1)} %collective-permute-done.12.refs_3_) | copy-start | bytes 786436
  131.7 32.9 %collective-permute-start.16 = (bf16[512,256]{1,0:T(8,128)(2,1)S(1)}, bf16[512,256]{1,0:T(8,128)(2,1)S(1)}, u32[]{:S(2)}, u32[]{:S(2)}) collective-permute-start(bf16[512,256]{1,0:T(8,128)(2,1)S(1)} %get-tuple-element.17), channel_id=1, source_target_pairs={{0,28},{1,20},{2,30},{3,22},{4,24},{5,16},{6,26},{7,18},{8,29},{9,... | collective-permute-start | bytes 786440 | tf_op jit(solution)/shard_map/ppermute | solution.py:357
  135.3 29.4 %copy-start.7 = (bf16[512,256]{1,0:T(8,128)(2,1)}, bf16[512,256]{1,0:T(8,128)(2,1)S(1)}, u32[]{:S(2)}) copy-start(bf16[512,256]{1,0:T(8,128)(2,1)S(1)} %collective-permute-done.13.refs_4_) | copy-start | bytes 786436
  135.3 29.3 %collective-permute-start.9 = (bf16[512,256]{1,0:T(8,128)(2,1)S(1)}, bf16[512,256]{1,0:T(8,128)(2,1)S(1)}, u32[]{:S(2)}, u32[]{:S(2)}) collective-permute-start(bf16[512,256]{1,0:T(8,128)(2,1)S(1)} %get-tuple-element.23), channel_id=1, source_target_pairs={{0,0},{1,8},{2,2},{3,10},{4,4},{5,12},{6,6},{7,14},{8,1},{9,9},{10... | collective-permute-start | bytes 786440 | tf_op jit(solution)/shard_map/ppermute | solution.py:357
  154.4 10.3 %copy-start.8 = (bf16[512,256]{1,0:T(8,128)(2,1)}, bf16[512,256]{1,0:T(8,128)(2,1)S(1)}, u32[]{:S(2)}) copy-start(bf16[512,256]{1,0:T(8,128)(2,1)S(1)} %collective-permute-done.14.refs_5_) | copy-start | bytes 786436
  161.3 3.4 %copy-start.9 = (bf16[512,256]{1,0:T(8,128)(2,1)}, bf16[512,256]{1,0:T(8,128)(2,1)S(1)}, u32[]{:S(2)}) copy-start(bf16[512,256]{1,0:T(8,128)(2,1)S(1)} %collective-permute-done.15.refs_6_) | copy-start | bytes 786436
  164.6 0.7 copy-start.10
  164.6 0.8 copy-start.11
  164.6 1.1 copy-start.3
  190.3 9.4 %all-to-all-start.2 = ((f32[4,32,512]{2,1,0:T(8,128)}), f32[4,32,512]{2,1,0:T(8,128)S(1)}, u32[]{:S(2)}, u32[]{:S(2)}) async-start(f32[4,32,512]{2,1,0:T(8,128)} %get-tuple-element.13), calls=%async_computation.2 | async-start | bytes 524288 | tf_op jit(solution)/shard_map/all_to_all | solution.py:314
